TPU v7x, 32 devices: a whole 2x2x4 slice. The times are simulated.
32 devices in a mesh: grp: 2 (over y), fs: 4 (over z), tp: 4 (over x, core).
Axes of the slice: x: 2, y: 2, z: 4, core: 2. Of those that a mesh axis runs over, the one named last changes fastest.
Arguments:
- tokens: bfloat16 [1536, 2048], P(('grp', 'tp')), parts along dimension 0, may hold values from -6 to 6
- routes: int32 [1536, 2], P(('grp', 'tp')), parts along dimension 0, may hold values from 0 to 3, all different within a row; in each aligned block of 192 rows (0 to 191, 192 to 383, ...) at most 128 rows name the same one
- route_weight: float32 [1536, 2], P(('grp', 'tp')), parts along dimension 0, may hold values from 0.2 to 1
- norm_gain: float32 [2048], P('fs'), may hold values from 0.1 to 1.9
- gate_train: float32 [4, 2048, 5632], P('tp', 'fs'), may hold values from -0.125 to 0.125
- up_train: float32 [4, 2048, 5632], P('tp', 'fs'), may hold values from -0.125 to 0.125
- down_train: float32 [4, 5632, 2048], P('tp', None, 'fs'), may hold values from -0.109375 to 0.109375
Outputs:
- gate_serve: bfloat16 [8, 2048, 5632], P(('grp', 'tp'), None, 'fs'), parts along dimension 0
- up_serve: bfloat16 [8, 2048, 5632], P(('grp', 'tp'), None, 'fs'), parts along dimension 0
- down_serve: bfloat16 [8, 5632, 2048], P(('grp', 'tp'), 'fs'), parts along dimension 0
- mixed: bfloat16 [1536, 2048], P(('grp', 'tp'), 'fs'), parts along dimension 0
There are 2 independent parts, one for each index of `grp`. A program takes and returns all parts, laid end to end along the dimension named above; an argument that names none is the same for every part. Nothing has to cross between parts.
Inputs may be any that keep to these rules, and one draw needn't show every extreme that they name: `routes`: each row names 2 different experts. In each aligned block of 192 rows no expert is named by more than 128 rows, a bound that some block reaches.
All inputs are finite; a program needn't handle non-finite values.
Results may differ from a plain program's by a relative error of at most 0.0087.
Values may be sent and summed in bfloat16 or wider, within the bound.
A program may use at most 128 MiB of HBM per device.

v0:
```python
import jax
import jax.numpy as jnp
from jax import lax
from jax.sharding import PartitionSpec as P

EXPERTS = 4
CAP = 128


def shards(tokens, routes, route_weight, norm_gain, gate_train, up_train, down_train):
    fs_count = lax.axis_size("fs")
    pieces = min(fs_count, 32)
    copies = fs_count // pieces
    gain_column = norm_gain[:, None]
    gate_low = (gate_train[0] * gain_column).astype(jnp.bfloat16)
    up_low = (up_train[0] * gain_column).astype(jnp.bfloat16)
    down_low = down_train[0].astype(jnp.bfloat16)
    gate_wide = jnp.tile(gate_low, (1, copies))
    up_wide = jnp.tile(up_low, (1, copies))
    down_wide = jnp.tile(down_low, (copies, 1))
    gate_new, up_new = (
        lax.all_to_all(gate_wide, "fs", split_axis=1, concat_axis=0, tiled=True),
        lax.all_to_all(up_wide, "fs", split_axis=1, concat_axis=0, tiled=True),
    )
    down_new = lax.all_to_all(down_wide, "fs", split_axis=0, concat_axis=1, tiled=True)
    tok_float = tokens.astype(jnp.float32)
    normed = (
        tok_float * lax.rsqrt(jnp.mean(tok_float * tok_float, axis=-1, keepdims=True) + 1e-06)
    ).astype(jnp.bfloat16)
    chosen = routes.reshape(-1)
    chosen_hot = (chosen[:, None] == jnp.arange(EXPERTS, dtype=jnp.int32)[None, :]).astype(
        jnp.int32
    )
    before = jnp.cumsum(chosen_hot, axis=0) - chosen_hot
    slot_rank = jnp.sum(before * chosen_hot, axis=1)
    slot_index = (chosen * CAP + slot_rank).reshape(routes.shape)
    slot_range = jnp.arange(EXPERTS * CAP, dtype=jnp.int32)
    select_rows = jnp.any(slot_range[:, None, None] == slot_index[None, :, :], axis=-1).astype(
        jnp.bfloat16
    )
    outgoing = jnp.dot(select_rows, normed, preferred_element_type=jnp.float32).astype(jnp.bfloat16)
    outgoing = outgoing.reshape(EXPERTS, CAP, normed.shape[1])
    arrived = lax.all_to_all(outgoing, "tp", split_axis=0, concat_axis=0, tiled=True).reshape(
        EXPERTS * CAP, normed.shape[1]
    )
    slot_count = EXPERTS * CAP // copies
    copy_index = lax.axis_index("fs") // pieces
    my_rows = lax.dynamic_slice_in_dim(arrived, copy_index * slot_count, slot_count, 0)
    gated = jnp.dot(my_rows, gate_new, preferred_element_type=jnp.float32)
    lifted = jnp.dot(my_rows, up_new, preferred_element_type=jnp.float32)
    hidden = (jax.nn.silu(gated) * lifted).astype(jnp.bfloat16)
    partial_out = jnp.dot(hidden, down_new, preferred_element_type=jnp.float32)
    placed = jnp.zeros((EXPERTS * CAP, partial_out.shape[1]), jnp.float32)
    placed = lax.dynamic_update_slice_in_dim(placed, partial_out, copy_index * slot_count, 0)
    expert_out = lax.psum_scatter(placed, "fs", scatter_dimension=1, tiled=True).astype(
        jnp.bfloat16
    )
    returned = lax.all_to_all(
        expert_out.reshape(EXPERTS, CAP, expert_out.shape[1]),
        "tp",
        split_axis=0,
        concat_axis=0,
        tiled=True,
    )
    returned = returned.reshape(EXPERTS * CAP, expert_out.shape[1]).astype(jnp.float32)
    blend_weight = jnp.sum(
        jnp.where(
            slot_range[None, None, :] == slot_index[:, :, None], route_weight[:, :, None], 0.0
        ),
        axis=1,
    )
    mixed = jnp.dot(
        blend_weight, returned, precision=lax.Precision.HIGHEST, preferred_element_type=jnp.float32
    )
    return (gate_new[None], up_new[None], down_new[None], mixed.astype(jnp.bfloat16))


def solution(mesh):
    in_specs = (
        P(("grp", "tp"), None),
        P(("grp", "tp"), None),
        P(("grp", "tp"), None),
        P("fs"),
        P("tp", "fs", None),
        P("tp", "fs", None),
        P("tp", None, "fs"),
    )
    out_specs = (
        P(("grp", "tp"), None, "fs"),
        P(("grp", "tp"), None, "fs"),
        P(("grp", "tp"), "fs", None),
        P(("grp", "tp"), "fs"),
    )
    return jax.shard_map(shards, mesh=mesh, in_specs=in_specs, out_specs=out_specs, check_vma=False)
```

profile of v0, /device:TPU:13, one launch (start us, length us, event | category | flops | bytes accessed | tf_op | source)
XLA Modules:
  0.0 586.1 jit_solution(4837379173826643466)
XLA Ops:
  7.2 0.8 copy.54
  8.3 1.2 reduce-window.6
  11.1 1.4 fusion.3
  12.4 3.3 convolution_convert_fusion
  15.7 4.3 all-to-all-start.3
  20.0 14.5 %squeeze.7 = f32[512,4,1408]{2,1,0:T(4,128)} reshape(f32[1,512,5632]{2,1,0:T(8,128)} %param.11) | data formatting | bytes 23068672 | tf_op jit(solution)/shard_map/squeeze | solution.py:15
  34.5 14.5 %squeeze.8 = f32[512,4,1408]{2,1,0:T(4,128)} reshape(f32[1,512,5632]{2,1,0:T(8,128)} %param.12) | data formatting | bytes 23068672 | tf_op jit(solution)/shard_map/squeeze | solution.py:16
  49.0 16.8 %fusion = (bf16[512,4,1408]{2,0,1:T(8,128)(2,1)}, bf16[512,4,1408]{2,0,1:T(8,128)(2,1)}) fusion(f32[512,4,1408]{2,1,0:T(4,128)} %squeeze.8, f32[512]{0:T(512)S(1)} %copy-done, f32[512,4,1408]{2,1,0:T(4,128)} %squeeze.7), kind=kLoop, calls=%fused_computation.1 | loop fusion | flops 11534336 | bytes 34605056 | tf_op jit(solution)/shard_map/convert_element_type | solution.py:16
  65.9 5.3 all-to-all-start
  71.1 7.5 %convert_element_type.44 = bf16[1,5632,512]{2,1,0:T(8,128)(2,1)} convert(f32[1,5632,512]{2,1,0:T(8,128)} %param.13) | non-fusion elementwise | flops 2883584 | bytes 17301504 | tf_op jit(solution)/shard_map/convert_element_type | solution.py:17
  78.7 116.4 %all-to-all-done = bf16[512,4,1408]{2,0,1:T(8,128)(2,1)} async-done(((bf16[512,4,1408]{2,0,1:T(8,128)(2,1)}), bf16[512,4,1408]{2,0,1:T(8,128)(2,1)}, u32[]{:S(2)}, u32[]{:S(2)}) %all-to-all-start) | async-done | bytes 5767200 | tf_op jit(solution)/shard_map/all_to_all | solution.py:22
  195.0 134.1 %all_to_all.58 = bf16[4,1408,512]{2,1,0:T(8,128)(2,1)} all-to-all(bf16[4,1408,512]{2,1,0:T(8,128)(2,1)} %bitcast.49), channel_id=1, replica_groups=mesh['grp'=2,'fs'=4,'tp'=4] {'fs'}, dimensions={0} | all-to-all | bytes 11534336 | tf_op jit(solution)/shard_map/all_to_all | solution.py:25
  329.1 7.0 %all-to-all-start.1 = ((bf16[512,4,1408]{2,0,1:T(8,128)(2,1)}), bf16[512,4,1408]{2,0,1:T(8,128)(2,1)}, u32[]{:S(2)}, u32[]{:S(2)}) async-start(bf16[512,4,1408]{2,0,1:T(8,128)(2,1)} %get-tuple-element.16), calls=%async_computation.1 | async-start | bytes 11534336 | tf_op jit(solution)/shard_map/all_to_all | solution.py:23
  336.1 8.3 %copy.53 = bf16[4,1408,512]{1,2,0:T(8,128)(2,1)} copy(bf16[4,1408,512]{2,1,0:T(8,128)(2,1)} %all_to_all.58) | data formatting | bytes 11534336 | tf_op jit(solution)/shard_map/all_to_all | solution.py:25
  344.4 7.6 %fusion.14 = f32[512,1408]{1,0:T(8,128)} fusion(bf16[512,2048]{1,0:T(8,128)(2,1)S(1)} %bitcast.50, bf16[2048,1408]{1,0:T(8,128)(2,1)} %bitcast.10), kind=kOutput, calls=%fused_computation.30 | convolution fusion | flops 2952790016 | bytes 10747904 | tf_op jit(solution)/shard_map/dot_general | solution.py:49
  352.0 106.6 %all-to-all-done.1 = bf16[512,4,1408]{2,0,1:T(8,128)(2,1)} async-done(((bf16[512,4,1408]{2,0,1:T(8,128)(2,1)}), bf16[512,4,1408]{2,0,1:T(8,128)(2,1)}, u32[]{:S(2)}, u32[]{:S(2)}) %all-to-all-start.1) | async-done | bytes 5767200 | tf_op jit(solution)/shard_map/all_to_all | solution.py:23
  458.6 13.9 %fusion.8 = f32[512,2048]{1,0:T(8,128)} fusion(bf16[1408,2048]{0,1:T(8,128)(2,1)} %bitcast.47, bf16[512,2048]{1,0:T(8,128)(2,1)S(1)} %bitcast.51, bf16[2048,1408]{1,0:T(8,128)(2,1)} %bitcast.11, f32[512,1408]{1,0:T(8,128)} %fusion.14), kind=kOutput, calls=%fused_computation.17 | convolution fusion | flops 5909905408 | bytes 20709376 | tf_op jit(solution)/shard_map/dot_general | solution.py:52
  472.6 79.6 %reduce-scatter.2.cloned.1.call-done = f32[512,512]{1,0:T(8,128)} async-done(((f32[512,2048]{1,0:T(8,128)}), f32[512,512]{1,0:T(8,128)}) %reduce-scatter.2.cloned.1.call-update) | async-done | bytes 1048592 | tf_op jit(solution)/shard_map/reduce_scatter | solution.py:55
  552.2 2.1 convert_element_type.52
  554.3 4.2 all-to-all-start.4
  558.6 8.2 %copy.57 = bf16[1,1408,2048]{2,1,0:T(8,128)(2,1)} copy(bf16[1,1408,2048]{1,2,0:T(8,128)(2,1)} %bitcast.48) | data formatting | bytes 11534336
  566.9 1.2 convolution_convert_fusion.1
  568.0 5.6 copy.68
  573.6 5.6 copy.69
  (21 shorter events, 2.0 us)
Async XLA Ops:
  15.7 50.2 %all-to-all-start.3 = ((bf16[4,128,2048]{2,1,0:T(8,128)(2,1)}), bf16[4,128,2048]{2,1,0:T(8,128)(2,1)S(1)}, u32[]{:S(2)}, u32[]{:S(2)}) async-start(bf16[4,128,2048]{2,1,0:T(8,128)(2,1)} %bitcast.8), calls=%async_computation.3 | async-start | bytes 4194304 | tf_op jit(solution)/shard_map/all_to_all | solution.py:43
  34.5 14.5 %copy-start = (f32[512]{0:T(512)S(1)}, f32[512]{0:T(512)}, u32[]{:S(2)}) copy-start(f32[512]{0:T(512)} %param.10) | copy-start | bytes 6148
  65.9 129.2 %all-to-all-start = ((bf16[512,4,1408]{2,0,1:T(8,128)(2,1)}), bf16[512,4,1408]{2,0,1:T(8,128)(2,1)}, u32[]{:S(2)}, u32[]{:S(2)}) async-start(bf16[512,4,1408]{2,0,1:T(8,128)(2,1)} %get-tuple-element.17), calls=%async_computation | async-start | bytes 11534336 | tf_op jit(solution)/shard_map/all_to_all | solution.py:22
  329.1 129.5 %all-to-all-start.1 = ((bf16[512,4,1408]{2,0,1:T(8,128)(2,1)}), bf16[512,4,1408]{2,0,1:T(8,128)(2,1)}, u32[]{:S(2)}, u32[]{:S(2)}) async-start(bf16[512,4,1408]{2,0,1:T(8,128)(2,1)} %get-tuple-element.16), calls=%async_computation.1 | async-start | bytes 11534336 | tf_op jit(solution)/shard_map/all_to_all | solution.py:23
  336.1 216.1 %reduce-scatter.2.cloned.1.call-start = ((), (), s32[]{:S(2)}) async-start(), calls=%async_computation.6 | async-start | bytes 5242880 | tf_op jit(solution)/shard_map/reduce_scatter | solution.py:55
  472.5 85.9 %copy-start.1 = (f32[192,2]{0,1:T(2,128)S(1)}, f32[192,2]{0,1:T(2,128)}, u32[]{:S(2)}) copy-start(f32[192,2]{0,1:T(2,128)} %param.9) | copy-start | bytes 4612
  554.3 12.6 %all-to-all-start.4 = ((bf16[4,128,512]{2,1,0:T(8,128)(2,1)}), bf16[4,128,512]{2,1,0:T(8,128)(2,1)S(1)}, u32[]{:S(2)}, u32[]{:S(2)}) async-start(bf16[4,128,512]{2,1,0:T(8,128)(2,1)} %bitcast.13), calls=%async_computation.5 | async-start | bytes 1048576 | tf_op jit(solution)/shard_map/all_to_all | solution.py:58
Sparse Core Ops, SparseCore 0:
  472.7 79.4 reduce-scatter.1
where the time goes:
time: 589 us; the launch traced here: 586 us
  waiting for transfers between devices  303 us (51%)
  blocking collectives  134 us (23%)
  local copies, waits for them, and re-layouts  58.3 us (10%)
  other arithmetic  30.4 us (5%)
  matrix products  25.9 us (4%)
  starting transfers between devices  20.7 us (4%)
  between operations  14.1 us (2%)
    all_to_all x1, blocking collectives, shards(): lax.all_to_all(down_wide, 'fs', split_axis=0, concat_axis=1, tiled=True)  134 us
    all_to_all x1, waiting for transfers between devices, shards(): lax.all_to_all(gate_wide, 'fs', split_axis=1, concat_axis=0, tiled=True)  116 us
    all_to_all x1, waiting for transfers between devices, shards(): lax.all_to_all(up_wide, 'fs', split_axis=1, concat_axis=0, tiled=True)  107 us
    reduce_scatter x1, waiting for transfers between devices, shards(): lax.psum_scatter(placed, 'fs', scatter_dimension=1, tiled=True)  79.6 us
    unnamed x8, local copies, waits for them, and re-layouts  20.2 us
    convert_element_type x1, other arithmetic, shards(): up_low = (up_train[0] * gain_column).astype(jnp.bfloat16)  16.8 us
    squeeze x1, local copies, waits for them, and re-layouts, shards(): gate_low = (gate_train[0] * gain_column).astype(jnp.bfloat16)  14.5 us
    squeeze x1, local copies, waits for them, and re-layouts, shards(): up_low = (up_train[0] * gain_column).astype(jnp.bfloat16)  14.5 us
  transfers between devices with their start and end apart: 5, of which 3 were waited for; matrix products, arithmetic and copies ran while one was open for 13% of the time, Pallas kernels for 0%

commit v1 on v0

--- a/solution.py
+++ b/solution.py
@@ -1,10 +1,266 @@
+import functools
 import jax
 import jax.numpy as jnp
 from jax import lax
+from jax.experimental import pallas as pl
+from jax.experimental.pallas import tpu as pltpu
 from jax.sharding import PartitionSpec as P
 
 EXPERTS = 4
 CAP = 128
+MESH = pl.DeviceIdType.MESH
+
+
+def exchange_kernel(F, T, R, C, gl, ul, dl, xs, bh, bl, go, uo, do, mo,
+                    gw, uw, dw, arr, gacc, uacc, hid, pbf, ret, msend, mown, mrecv,
+                    zs, zr, ys, yr, ts, tr, ps, pr, ms, mr, loc, xloc, osem):
+    g, f, t = lax.axis_index("grp"), lax.axis_index("fs"), lax.axis_index("tp")
+    H = R // 2
+    lows, wins, outs = (gl, ul, dl), (gw, uw, dw), (go, uo, do)
+    half_f = F // 2
+    lo = lax.div(f, half_f)
+    peers = [lax.rem(t + d, T) for d in range(1, T)]
+    others = [lo * k + (1 - lo) * (F - 1 - k) for k in range(half_f)]
+    others += [lo * half_f + lax.rem(f - lo * half_f + 1 + j, half_f) for j in range(half_f - 1)]
+
+    barrier = pltpu.get_barrier_semaphore()
+    for p in peers:
+        pl.semaphore_signal(barrier, inc=1, device_id={"tp": p}, device_id_type=MESH)
+    for p in others:
+        pl.semaphore_signal(barrier, inc=1, device_id={"fs": p}, device_id_type=MESH)
+    pl.semaphore_signal(barrier, inc=1, device_id={"grp": 1 - g}, device_id_type=MESH)
+    pl.semaphore_wait(barrier, len(peers) + len(others) + 1)
+
+    def cols_of(src, half):
+        return pl.ds(pl.multiple_of(src * R + half * H, H), H)
+
+    def part(a, src, half):
+        if a < 2:
+            return wins[a].at[cols_of(src, half), :]
+        return dw.at[:, cols_of(src, half)]
+
+    def z_copy(a, tgt, src):
+        if a < 2:
+            piece = lows[a].at[pl.ds(pl.multiple_of(g * H, H), H), pl.ds(pl.multiple_of(tgt * C, C), C)]
+        else:
+            piece = dl.at[pl.ds(pl.multiple_of(tgt * C, C), C), pl.ds(pl.multiple_of(g * H, H), H)]
+        return pltpu.make_async_remote_copy(
+            src_ref=piece, dst_ref=part(a, src, g), send_sem=zs.at[a, tgt], recv_sem=zr.at[a, src],
+            device_id={"fs": tgt}, device_id_type=MESH)
+
+    def z_recv(a, src):
+        return pltpu.make_async_remote_copy(
+            src_ref=part(a, src, g), dst_ref=part(a, src, g), send_sem=zs.at[a, src], recv_sem=zr.at[a, src],
+            device_id={"fs": src}, device_id_type=MESH)
+
+    def y_copy(a, src, half):
+        return pltpu.make_async_remote_copy(
+            src_ref=part(a, src, half), dst_ref=part(a, src, half), send_sem=ys.at[a, src], recv_sem=yr.at[a, src],
+            device_id={"grp": 1 - g}, device_id_type=MESH)
+
+    def slots(q):
+        return pl.ds(pl.multiple_of(q * CAP, CAP), CAP)
+
+    def t_copy(tgt, src):
+        return pltpu.make_async_remote_copy(
+            src_ref=xs.at[tgt], dst_ref=arr.at[slots(src), :], send_sem=ts.at[tgt], recv_sem=tr.at[src],
+            device_id={"tp": tgt}, device_id_type=MESH)
+
+    def p_copy(c, half, tgt, src):
+        cols = cols_of(c, half)
+        return pltpu.make_async_remote_copy(
+            src_ref=pbf.at[slots(tgt), cols], dst_ref=ret.at[slots(src), cols],
+            send_sem=ps.at[c, half, tgt], recv_sem=pr.at[c, half, src],
+            device_id={"tp": tgt}, device_id_type=MESH)
+
+    def m_copy(tgt, half, src):
+        return pltpu.make_async_remote_copy(
+            src_ref=msend.at[:, cols_of(tgt, half)], dst_ref=mrecv.at[src, :, pl.ds(pl.multiple_of(half * H, H), H)],
+            send_sem=ms.at[tgt, half], recv_sem=mr.at[src, half],
+            device_id={"fs": tgt}, device_id_type=MESH)
+
+    def own_copy(a):
+        if a < 2:
+            return pltpu.make_async_copy(lows[a].at[:, pl.ds(pl.multiple_of(f * C, C), C)],
+                                         wins[a].at[pl.ds(pl.multiple_of(f * R, R), R), :], loc.at[a])
+        return pltpu.make_async_copy(dl.at[pl.ds(pl.multiple_of(f * C, C), C), :],
+                                     dw.at[:, pl.ds(pl.multiple_of(f * R, R), R)], loc.at[a])
+
+    def out_copy(a, src):
+        whole = pl.ds(pl.multiple_of(src * R, R), R)
+        if a < 2:
+            return pltpu.make_async_copy(wins[a].at[whole, :], outs[a].at[whole, :], osem.at[a, src])
+        return pltpu.make_async_copy(dw.at[:, whole], do.at[:, whole], osem.at[a, src])
+
+    for p in peers:
+        t_copy(p, t).start()
+    for a in (0, 1):
+        for p in others:
+            z_copy(a, p, f).start()
+    for p in others:
+        z_copy(2, p, f).start()
+    own_x = pltpu.make_async_copy(xs.at[t], arr.at[slots(t), :], xloc.at[0])
+    own_x.start()
+    for a in range(3):
+        own_copy(a).start()
+
+    rows_all = arr.shape[0]
+    M = min(256, rows_all)
+
+    def multiply(a, src, first):
+        acc = (gacc, uacc)[a]
+        deep = pl.ds(pl.multiple_of(src * R, R), R)
+
+        @pl.loop(0, rows_all // M)
+        def _(m):
+            rows = pl.ds(pl.multiple_of(m * M, M), M)
+            value = jnp.dot(arr[rows, deep], wins[a][deep, :], preferred_element_type=jnp.float32)
+            if first:
+                acc[rows, :] = value
+            else:
+                acc[rows, :] += value
+
+    def activate():
+        @pl.loop(0, rows_all // 64)
+        def _(m):
+            rows = pl.ds(pl.multiple_of(m * 64, 64), 64)
+            v = gacc[rows, :]
+            hid[rows, :] = (v / (1.0 + jnp.exp(-v)) * uacc[rows, :]).astype(jnp.bfloat16)
+
+    def partial_out(src, half):
+        cols = cols_of(src, half)
+
+        @pl.loop(0, rows_all // M)
+        def _(m):
+            rows = pl.ds(pl.multiple_of(m * M, M), M)
+            pbf[rows, cols] = jnp.dot(hid[rows, :], dw[:, cols], preferred_element_type=jnp.float32).astype(jnp.bfloat16)
+
+        for p in peers:
+            p_copy(src, half, p, t).start()
+        ret[slots(t), cols] = pbf[slots(t), cols]
+
+    def mix(src, half, own):
+        cols = cols_of(src, half)
+        for p in peers:
+            p_copy(src, half, p, p).wait_recv()
+        value = jnp.dot(bh[...], ret[:, cols], preferred_element_type=jnp.float32) + jnp.dot(
+            bl[...], ret[:, cols], preferred_element_type=jnp.float32)
+        if own:
+            mown[:, pl.ds(pl.multiple_of(half * H, H), H)] = value
+        else:
+            msend[:, cols] = value.astype(jnp.bfloat16)
+            m_copy(src, half, f).start()
+
+    own_x.wait()
+    for p in peers:
+        t_copy(p, p).wait_recv()
+    for a in (0, 1):
+        own_copy(a).wait()
+        out_copy(a, f).start()
+        multiply(a, f, True)
+    own_copy(2).wait()
+    out_copy(2, f).start()
+
+    pending = []
+
+    def submit(src, half, own):
+        partial_out(src, half)
+        pending.append((src, half, own))
+        if len(pending) > 1:
+            mix(*pending.pop(0))
+
+    def finish(a, src):
+        y_copy(a, src, 1 - g).wait_recv()
+        out_copy(a, src).start()
+        if a < 2:
+            multiply(a, src, False)
+        else:
+            submit(src, 1 - g, False)
+
+    items = [(a, src) for a in (0, 1) for src in others] + [(2, src) for src in others]
+    last = None
+    for i, (a, src) in enumerate(items):
+        z_recv(a, src).wait_recv()
+        y_copy(a, src, g).start()
+        if last is not None:
+            finish(*last)
+            if i == 2 * len(others):
+                activate()
+                submit(f, 0, True)
+                submit(f, 1, True)
+        if a == 2:
+            submit(src, g, False)
+        last = (a, src)
+    finish(*last)
+    for entry in pending:
+        mix(*entry)
+    total = mown[...]
+    for p in others:
+        for half in range(2):
+            m_copy(p, half, p).wait_recv()
+        total = total + mrecv[p].astype(jnp.float32)
+    mo[...] = total.astype(jnp.bfloat16)
+
+    for p in peers:
+        t_copy(p, t).wait_send()
+        for c in range(F):
+            for half in range(2):
+                p_copy(c, half, p, t).wait_send()
+    for p in others:
+        for a in range(3):
+            z_copy(a, p, f).wait_send()
+            y_copy(a, p, g).wait_send()
+        for half in range(2):
+            m_copy(p, half, f).wait_send()
+    for a in range(3):
+        for c in range(F):
+            out_copy(a, c).wait()
+
+
+def exchange(F, T, gl, ul, dl, xs, bh, bl):
+    R, FF = gl.shape
+    C = FF // F
+    D = F * R
+    S = xs.shape[0] * xs.shape[1]
+    tok = bh.shape[0]
+    bf, f32 = jnp.bfloat16, jnp.float32
+    any_spec, vm = pl.BlockSpec(memory_space=pl.ANY), pl.BlockSpec(memory_space=pltpu.VMEM)
+    dma = pltpu.SemaphoreType.DMA
+    return pl.pallas_call(
+        functools.partial(exchange_kernel, F, T, R, C),
+        name="exchange",
+        out_shape=(jax.ShapeDtypeStruct((D, C), bf), jax.ShapeDtypeStruct((D, C), bf),
+                   jax.ShapeDtypeStruct((C, D), bf), jax.ShapeDtypeStruct((tok, R), bf)),
+        in_specs=[any_spec] * 4 + [vm] * 2,
+        out_specs=(any_spec, any_spec, any_spec, vm),
+        scratch_shapes=[
+            pltpu.VMEM((D, C), bf), pltpu.VMEM((D, C), bf), pltpu.VMEM((C, D), bf), pltpu.VMEM((S, D), bf),
+            pltpu.VMEM((S, C), f32), pltpu.VMEM((S, C), f32), pltpu.VMEM((S, C), bf),
+            pltpu.VMEM((S, D), bf), pltpu.VMEM((S, D), bf), pltpu.VMEM((tok, D), bf),
+            pltpu.VMEM((tok, R), f32), pltpu.VMEM((F, tok, R), bf),
+            dma((3, F)), dma((3, F)), dma((3, F)), dma((3, F)), dma((T,)), dma((T,)),
+            dma((F, 2, T)), dma((F, 2, T)), dma((F, 2)), dma((F, 2)), dma((3,)), dma((1,)), dma((3, F)),
+        ],
+        compiler_params=pltpu.CompilerParams(collective_id=0, has_side_effects=True, vmem_limit_bytes=60 * 1024 * 1024),
+    )(gl, ul, dl, xs, bh, bl)
+
+
+def fits(grp_count, fs_count, pieces, gate_train):
+    rows, wide = gate_train.shape[1:]
+    return (grp_count == 2 and fs_count == pieces and fs_count % 2 == 0
+            and wide % (fs_count * 128) == 0 and rows % 256 == 0)
+
+
+def swapped(gate_low, up_low, down_low, copies):
+    gate_wide = jnp.tile(gate_low, (1, copies))
+    up_wide = jnp.tile(up_low, (1, copies))
+    down_wide = jnp.tile(down_low, (copies, 1))
+    gate_new, up_new = (
+        lax.all_to_all(gate_wide, "fs", split_axis=1, concat_axis=0, tiled=True),
+        lax.all_to_all(up_wide, "fs", split_axis=1, concat_axis=0, tiled=True),
+    )
+    down_new = lax.all_to_all(down_wide, "fs", split_axis=0, concat_axis=1, tiled=True)
+    return gate_new, up_new, down_new
 
 
 def shards(tokens, routes, route_weight, norm_gain, gate_train, up_train, down_train):
@@ -15,14 +271,9 @@
     gate_low = (gate_train[0] * gain_column).astype(jnp.bfloat16)
     up_low = (up_train[0] * gain_column).astype(jnp.bfloat16)
     down_low = down_train[0].astype(jnp.bfloat16)
-    gate_wide = jnp.tile(gate_low, (1, copies))
-    up_wide = jnp.tile(up_low, (1, copies))
-    down_wide = jnp.tile(down_low, (copies, 1))
-    gate_new, up_new = (
-        lax.all_to_all(gate_wide, "fs", split_axis=1, concat_axis=0, tiled=True),
-        lax.all_to_all(up_wide, "fs", split_axis=1, concat_axis=0, tiled=True),
-    )
-    down_new = lax.all_to_all(down_wide, "fs", split_axis=0, concat_axis=1, tiled=True)
+    fused = fits(lax.axis_size("grp"), fs_count, pieces, gate_train)
+    if not fused:
+        gate_new, up_new, down_new = swapped(gate_low, up_low, down_low, copies)
     tok_float = tokens.astype(jnp.float32)
     normed = (
         tok_float * lax.rsqrt(jnp.mean(tok_float * tok_float, axis=-1, keepdims=True) + 1e-06)
@@ -40,6 +291,20 @@
     )
     outgoing = jnp.dot(select_rows, normed, preferred_element_type=jnp.float32).astype(jnp.bfloat16)
     outgoing = outgoing.reshape(EXPERTS, CAP, normed.shape[1])
+    blend_weight = jnp.sum(
+        jnp.where(
+            slot_range[None, None, :] == slot_index[:, :, None], route_weight[:, :, None], 0.0
+        ),
+        axis=1,
+    )
+    if fused:
+        blend_high = lax.reduce_precision(blend_weight, 8, 7)
+        blend_low = (blend_weight - blend_high).astype(jnp.bfloat16)
+        blend_high = blend_high.astype(jnp.bfloat16)
+        gate_new, up_new, down_new, mixed = exchange(
+            fs_count, lax.axis_size("tp"), gate_low, up_low, down_low, outgoing, blend_high, blend_low
+        )
+        return (gate_new[None], up_new[None], down_new[None], mixed)
     arrived = lax.all_to_all(outgoing, "tp", split_axis=0, concat_axis=0, tiled=True).reshape(
         EXPERTS * CAP, normed.shape[1]
     )
@@ -63,12 +328,6 @@
         tiled=True,
     )
     returned = returned.reshape(EXPERTS * CAP, expert_out.shape[1]).astype(jnp.float32)
-    blend_weight = jnp.sum(
-        jnp.where(
-            slot_range[None, None, :] == slot_index[:, :, None], route_weight[:, :, None], 0.0
-        ),
-        axis=1,
-    )
     mixed = jnp.dot(
         blend_weight, returned, precision=lax.Precision.HIGHEST, preferred_element_type=jnp.float32
     )

time: 589 us -> 297 us (0.50)
  waiting for transfers between devices: 303 us -> 0 us
  Pallas kernels: 0 us -> 247 us
  blocking collectives: 134 us -> 0 us
  local copies, waits for them, and re-layouts: 58.3 us -> 15 us
  matrix products: 25.9 us -> 3.3 us
  starting transfers between devices: 20.7 us -> 0 us
  between operations: 14.1 us -> 0.71 us
    pallas_call x0 -> x1, Pallas kernels: none -> 247 us  [exchange(): pl.pallas_call(functools.partial(exchange_kernel, F, T, R, C), name='exch...]
    all_to_all x4 -> x0, waiting for transfers between devices: 223 us -> none  [the longest x1 116 us: shards(): lax.all_to_all(gate_wide, 'fs', split_axis=1, concat_axis=0, tiled=True)]
    all_to_all x1 -> x0, blocking collectives: 134 us -> none  [shards(): lax.all_to_all(down_wide, 'fs', split_axis=0, concat_axis=1, tiled=True)]
    reduce_scatter x1 -> x0, waiting for transfers between devices: 79.6 us -> none  [shards(): lax.psum_scatter(placed, 'fs', scatter_dimension=1, tiled=True)]
    squeeze x2 -> x0, local copies, waits for them, and re-layouts: 29.1 us -> none  [the longest x1 14.5 us: shards(): gate_low = (gate_train[0] * gain_column).astype(jnp.bfloat16)]
    dot_general x3 -> x0, matrix products: 22.7 us -> none  [the longest x1 13.9 us: shards(): partial_out = jnp.dot(hidden, down_new, preferred_element_type=jnp.float32)]
    all_to_all x4 -> x0, starting transfers between devices: 20.7 us -> none  [the longest x1 6.99 us: shards(): lax.all_to_all(up_wide, 'fs', split_axis=1, concat_axis=0, tiled=True)]
    all_to_all x1 -> x0, local copies, waits for them, and re-layouts: 8.33 us -> none  [shards(): lax.all_to_all(down_wide, 'fs', split_axis=0, concat_axis=1, tiled=True)]
  transfers between devices with their start and end apart: 5 -> 0, of which waited for: 3 -> 0; matrix products, arithmetic and copies ran while one was open for 13% -> 0% of each run, Pallas kernels for 0% -> 0%
where the time goes in v1:
time: 297 us; the launch traced here: 292 us
  Pallas kernels  247 us (83%)
  other arithmetic  26.1 us (9%)
  local copies, waits for them, and re-layouts  15 us (5%)
  matrix products  3.3 us (1%)
    pallas_call x1, Pallas kernels, exchange(): pl.pallas_call(functools.partial(exchange_kernel, F, T, R, C), name='exch...  247 us
    unnamed x15, local copies, waits for them, and re-layouts  14.3 us
    convert_element_type x1, other arithmetic, shards(): up_low = (up_train[0] * gain_column).astype(jnp.bfloat16)  13.2 us
    convert_element_type x1, other arithmetic, shards(): down_low = down_train[0].astype(jnp.bfloat16)  7.56 us

profile of v1, /device:TPU:13, one launch (start us, length us, event | category | flops | bytes accessed | tf_op | source)
XLA Modules:
  0.0 292.2 jit_solution(6586744406867779318)
XLA Ops:
  0.6 1.4 fusion.2
  2.0 0.8 copy.25
  2.8 0.1 eq.56
  3.0 0.1 eq.52
  3.1 1.2 reduce-window.6
  4.3 0.2 slice_reduce_fusion
  4.6 0.2 reduce-window.9
  4.7 0.1 add_bitcast_fusion
  4.8 0.1 reduce_sum.30
  5.0 0.1 copy.27
  5.1 0.7 multiply_add_fusion
  5.8 0.1 fusion.6
  5.9 0.9 select_reduce_fusion
  6.8 0.8 fusion.7
  7.6 3.3 %convolution_convert_fusion = bf16[512,2048]{1,0:T(8,128)(2,1)} fusion(pred[512,192]{0,1:T(8,128)(4,1)S(1)} %fusion.6, bf16[192,2048]{1,0:T(8,128)(2,1)} %param.7, f32[192]{0:T(256)S(1)} %add_rsqrt_fusion), kind=kOutput, calls=%fused_computation.5 | convolution fusion | flops 404881408 | bytes 2982656 | tf_op jit(solution)/shard_map/dot_general | solution.py:292
  10.9 7.6 %convert_bitcast_fusion.dl = bf16[5632,512]{1,0:T(8,128)(2,1)} fusion(f32[1,5632,512]{2,1,0:T(8,128)} %param.13), kind=kLoop, calls=%fused_computation.4 | loop fusion | flops 2883584 | bytes 17301504 | tf_op jit(solution)/shard_map/convert_element_type | solution.py:273
  18.4 13.2 %fusion = (bf16[512,5632]{1,0:T(8,128)(2,1)}, bf16[512,5632]{1,0:T(8,128)(2,1)}) fusion(f32[1,512,5632]{2,1,0:T(8,128)} %param.12, f32[512]{0:T(512)S(1)} %copy-done.2, f32[1,512,5632]{2,1,0:T(8,128)} %param.11), kind=kLoop, calls=%fused_computation.1 | loop fusion | flops 11534336 | bytes 34605056 | tf_op jit(solution)/shard_map/convert_element_type | solution.py:272
  31.6 247.1 %exchange.1 = (bf16[2048,1408]{1,0:T(8,128)(2,1)}, bf16[2048,1408]{1,0:T(8,128)(2,1)}, bf16[1408,2048]{1,0:T(8,128)(2,1)}, bf16[192,512]{1,0:T(8,128)(2,1)}) custom-call(bf16[512,5632]{1,0:T(8,128)(2,1)} %get-tuple-element.15.gl, bf16[512,5632]{1,0:T(8,128)(2,1)} %get-tuple-element.14.ul, bf16[5632,512]{1,0:T(8,128)(2,1)} %convert_bitcast_fusion.dl, ...), custom_call_target="tpu_custom_call" | custom-call | tf_op jit(solution)/shard_map/exchange/pallas_call | solution.py:229
  278.7 0.0 slice-start
  278.7 6.1 %copy.34 = bf16[1,2048,1408]{2,1,0:T(8,128)(2,1)} copy(bf16[1,2048,1408]{2,1,0:T(8,128)(2,1)} %bitcast.39) | data formatting | bytes 11534336
  284.8 2.9 %copy.35 = bf16[1,2048,1408]{2,1,0:T(8,128)(2,1)} copy(bf16[1,2048,1408]{2,1,0:T(8,128)(2,1)S(1)} %bitcast.38) | data formatting | bytes 11534336
  287.8 1.2 slice-done.1
  289.0 2.5 copy.36
  291.5 0.7 copy.37
  (12 shorter events, 0.1 us)
Async XLA Ops:
  10.9 7.6 %copy-start.2 = (f32[512]{0:T(512)S(1)}, f32[512]{0:T(512)}, u32[]{:S(2)}) copy-start(f32[512]{0:T(512)} %param.10) | copy-start | bytes 6148
  278.7 6.2 %copy-start = (bf16[2048,1408]{1,0:T(8,128)(2,1)S(1)}, bf16[2048,1408]{1,0:T(8,128)(2,1)}, u32[]{:S(2)}) copy-start(bf16[2048,1408]{1,0:T(8,128)(2,1)} %get-tuple-element.9) | copy-start | bytes 17301508
  278.7 9.1 %slice-start = ((s8[5767168]{0:T(1024)(128)(4,1)}), s8[4194304]{0:T(1024)(128)(4,1)S(1)}, s32[]{:S(2)}) async-start(s8[5767168]{0:T(1024)(128)(4,1)} %bitcast.35), calls=%async_computation | async-start | bytes 8388608
  284.8 4.1 %slice-start.1 = ((s8[5767168]{0:T(1024)(128)(4,1)}), s8[1572864]{0:T(1024)(128)(4,1)S(1)}, s32[]{:S(2)}) async-start(s8[5767168]{0:T(1024)(128)(4,1)} %bitcast.35), calls=%async_computation.1 | async-start | bytes 3145728
  289.0 2.5 copy-start.1

commit v2 on v1

v2 whole, which is shorter than its diff:
```python
import functools
import jax
import jax.numpy as jnp
from jax import lax
from jax.experimental import pallas as pl
from jax.experimental.pallas import tpu as pltpu
from jax.sharding import PartitionSpec as P

EXPERTS = 4
CAP = 128
MESH = pl.DeviceIdType.MESH


def exchange_kernel(F, T, R, C, Q, gt, ut, dt, gain, tokens, routes, routes_t, weight, gw, uw, dw, mo,
                    wide, tall, sendw, sendt, normed, xs, bh, bl,
                    arr, gacc, uacc, hid, pbf, ret, msend, mown, mrecv,
                    zs, zr, ys, yr, ts, tr, ps, pr, ms, mr, loc):
    g, f, t = lax.axis_index("grp"), lax.axis_index("fs"), lax.axis_index("tp")
    H = R // 2
    wins = (gw, uw, dw)
    pieces_of = (1, 1, Q)
    half_f = F // 2
    lo = lax.div(f, half_f)
    peers = [lax.rem(t + d, T) for d in range(1, T)]
    others = [lo * k + (1 - lo) * (F - 1 - k) for k in range(half_f)]
    others += [lo * half_f + lax.rem(f - lo * half_f + 1 + j, half_f) for j in range(half_f - 1)]

    barrier = pltpu.get_barrier_semaphore()
    for p in peers:
        pl.semaphore_signal(barrier, inc=1, device_id={"tp": p}, device_id_type=MESH)
    for p in others:
        pl.semaphore_signal(barrier, inc=1, device_id={"fs": p}, device_id_type=MESH)
    pl.semaphore_signal(barrier, inc=1, device_id={"grp": 1 - g}, device_id_type=MESH)
    pl.semaphore_wait(barrier, len(peers) + len(others) + 1)

    def cols_of(src, half):
        return pl.ds(pl.multiple_of(src * R + half * H, H), H)

    def part(a, src, half, q):
        if a < 2:
            return wins[a].at[cols_of(src, half), :]
        return dw.at[pl.ds(q * (C // Q), C // Q), cols_of(src, half)]

    def z_copy(a, k, tgt, src, q):
        piece = sendw.at[a, k] if a < 2 else sendt.at[k, pl.ds(q * (C // Q), C // Q), :]
        return pltpu.make_async_remote_copy(
            src_ref=piece, dst_ref=part(a, src, g, q), send_sem=zs.at[a, k, q], recv_sem=zr.at[a, src, q],
            device_id={"fs": tgt}, device_id_type=MESH)

    def z_send(a, k):
        for q in range(pieces_of[a]):
            z_copy(a, k, others[k], f, q).start()

    def z_recv(a, src, q):
        return pltpu.make_async_remote_copy(
            src_ref=part(a, src, g, q), dst_ref=part(a, src, g, q), send_sem=zs.at[a, 0, q],
            recv_sem=zr.at[a, src, q], device_id={"fs": src}, device_id_type=MESH)

    def y_copy(a, src, half, q):
        return pltpu.make_async_remote_copy(
            src_ref=part(a, src, half, q), dst_ref=part(a, src, half, q), send_sem=ys.at[a, src, q],
            recv_sem=yr.at[a, src, q], device_id={"grp": 1 - g}, device_id_type=MESH)

    def slots(q):
        return pl.ds(pl.multiple_of(q * CAP, CAP), CAP)

    def t_copy(tgt, src):
        return pltpu.make_async_remote_copy(
            src_ref=xs.at[slots(tgt), :], dst_ref=arr.at[slots(src), :], send_sem=ts.at[tgt], recv_sem=tr.at[src],
            device_id={"tp": tgt}, device_id_type=MESH)

    def p_copy(c, half, tgt, src):
        cols = cols_of(c, half)
        return pltpu.make_async_remote_copy(
            src_ref=pbf.at[slots(tgt), cols], dst_ref=ret.at[slots(src), cols],
            send_sem=ps.at[c, half, tgt], recv_sem=pr.at[c, half, src],
            device_id={"tp": tgt}, device_id_type=MESH)

    def m_copy(tgt, half, src):
        return pltpu.make_async_remote_copy(
            src_ref=msend.at[:, cols_of(tgt, half)], dst_ref=mrecv.at[src, :, pl.ds(pl.multiple_of(half * H, H), H)],
            send_sem=ms.at[tgt, half], recv_sem=mr.at[src, half],
            device_id={"fs": tgt}, device_id_type=MESH)

    tasks = [(a, k, g) for a in range(3) for k in range(len(others))]
    tasks += [(a, None, half) for a in range(3) for half in range(2)]

    def stage_copy(n):
        a, k, half = tasks[n]
        tgt = f if k is None else others[k]
        near, far = pl.ds(pl.multiple_of(half * H, H), H), pl.ds(pl.multiple_of(tgt * C, C), C)
        if a < 2:
            return pltpu.make_async_copy((gt, ut)[a].at[near, far], wide.at[n % 3], loc.at[n % 3])
        return pltpu.make_async_copy(dt.at[far, near], tall.at[n % 3], loc.at[3 + n % 3])

    def cast(n):
        a, k, half = tasks[n]
        stage_copy(n).wait()
        if a < 2:
            @pl.loop(0, H // 32)
            def _(m):
                rows = pl.ds(pl.multiple_of(m * 32, 32), 32)
                scale = gain[pl.ds(pl.multiple_of(half * H + m * 32, 32), 32), :]
                value = (wide[n % 3, rows, :] * scale).astype(jnp.bfloat16)
                if k is None:
                    wins[a][pl.ds(pl.multiple_of(f * R + half * H + m * 32, 32), 32), :] = value
                else:
                    sendw[a, k, rows, :] = value
        else:
            @pl.loop(0, C // 128)
            def _(m):
                rows = pl.ds(pl.multiple_of(m * 128, 128), 128)
                value = tall[n % 3, rows, :].astype(jnp.bfloat16)
                if k is None:
                    dw[rows, cols_of(f, half)] = value
                else:
                    sendt[k, rows, :] = value
        if n + 3 < len(tasks):
            stage_copy(n + 3).start()

    def route():
        tok, slot_all = tokens.shape[0], arr.shape[0]

        @pl.loop(0, tok // 32)
        def _(m):
            rows = pl.ds(pl.multiple_of(m * 32, 32), 32)
            value = tokens[rows, :].astype(jnp.float32)
            normed[rows, :] = (
                value * lax.rsqrt(jnp.mean(value * value, axis=-1, keepdims=True) + 1e-06)
            ).astype(jnp.bfloat16)

        def ranks(shape, axis, one, two, hot_first, earlier):
            expert = lax.broadcasted_iota(jnp.int32, shape, axis)
            hot = jnp.where((expert == one) | (expert == two), 1.0, 0.0).astype(jnp.bfloat16)
            order = (hot, earlier) if hot_first else (earlier, hot)
            before = jnp.dot(*order, preferred_element_type=jnp.float32)
            return [
                name.astype(jnp.float32) * CAP
                + jnp.sum(jnp.where(expert == name, before, 0.0), axis=axis, keepdims=True)
                for name in (one, two)
            ]

        row = lax.broadcasted_iota(jnp.int32, (tok, tok), 0)
        col = lax.broadcasted_iota(jnp.int32, (tok, tok), 1)
        first, second = ranks((16, tok), 0, routes_t[0:1, :], routes_t[1:2, :], True,
                              jnp.where(row < col, 1.0, 0.0).astype(jnp.bfloat16))
        slot = lax.broadcasted_iota(jnp.int32, (slot_all, tok), 0).astype(jnp.float32)
        select = jnp.where((slot == first) | (slot == second), 1.0, 0.0).astype(jnp.bfloat16)
        for n in range(4):
            cols = pl.ds(n * (F * R // 4), F * R // 4)
            xs[:, cols] = jnp.dot(select, normed[:, cols], preferred_element_type=jnp.float32).astype(jnp.bfloat16)
        first, second = ranks((tok, 128), 1, routes[:, 0:1], routes[:, 1:2], False,
                              jnp.where(row > col, 1.0, 0.0).astype(jnp.bfloat16))
        slot = lax.broadcasted_iota(jnp.int32, (tok, slot_all), 1).astype(jnp.float32)
        blend = jnp.where(slot == first, weight[:, 0:1], 0.0) + jnp.where(slot == second, weight[:, 1:2], 0.0)
        high = blend.astype(jnp.bfloat16)
        bh[...] = high
        bl[...] = (blend - high.astype(jnp.float32)).astype(jnp.bfloat16)

    for n in range(3):
        stage_copy(n).start()
    remote = 3 * len(others)
    for n in range(remote):
        cast(n)
        if n > 0:
            z_send(*tasks[n - 1][:2])
    route()
    z_send(*tasks[remote - 1][:2])
    for n in range(remote, len(tasks)):
        cast(n)
        if n == remote:
            for p in peers:
                t_copy(p, t).start()
    arr[slots(t), :] = xs[slots(t), :]

    rows_all = arr.shape[0]
    M = min(256, rows_all)

    def multiply(a, src, first):
        acc = (gacc, uacc)[a]
        deep = pl.ds(pl.multiple_of(src * R, R), R)

        @pl.loop(0, rows_all // M)
        def _(m):
            rows = pl.ds(pl.multiple_of(m * M, M), M)
            value = jnp.dot(arr[rows, deep], wins[a][deep, :], preferred_element_type=jnp.float32)
            if first:
                acc[rows, :] = value
            else:
                acc[rows, :] += value

    def activate():
        @pl.loop(0, rows_all // 64)
        def _(m):
            rows = pl.ds(pl.multiple_of(m * 64, 64), 64)
            v = gacc[rows, :]
            hid[rows, :] = (v / (1.0 + jnp.exp(-v)) * uacc[rows, :]).astype(jnp.bfloat16)

    def partial_out(src, half):
        cols = cols_of(src, half)

        @pl.loop(0, rows_all // M)
        def _(m):
            rows = pl.ds(pl.multiple_of(m * M, M), M)
            pbf[rows, cols] = jnp.dot(hid[rows, :], dw[:, cols], preferred_element_type=jnp.float32).astype(jnp.bfloat16)

        for p in peers:
            p_copy(src, half, p, t).start()
        ret[slots(t), cols] = pbf[slots(t), cols]

    def mix(src, half, own):
        cols = cols_of(src, half)
        for p in peers:
            p_copy(src, half, p, p).wait_recv()
        value = jnp.dot(bh[...], ret[:, cols], preferred_element_type=jnp.float32) + jnp.dot(
            bl[...], ret[:, cols], preferred_element_type=jnp.float32)
        if own:
            mown[:, pl.ds(pl.multiple_of(half * H, H), H)] = value
        else:
            msend[:, cols] = value.astype(jnp.bfloat16)
            m_copy(src, half, f).start()

    for p in peers:
        t_copy(p, p).wait_recv()
    for a in (0, 1):
        multiply(a, f, True)

    pending = []

    def submit(src, half, own):
        partial_out(src, half)
        pending.append((src, half, own))
        if len(pending) > 1:
            mix(*pending.pop(0))

    def finish(a, src):
        for q in range(pieces_of[a]):
            y_copy(a, src, 1 - g, q).wait_recv()
        if a < 2:
            multiply(a, src, False)
        else:
            submit(src, 1 - g, False)

    items = [(a, src) for a in (0, 1) for src in others] + [(2, src) for src in others]
    last = None
    for i, (a, src) in enumerate(items):
        for q in range(pieces_of[a]):
            z_recv(a, src, q).wait_recv()
            y_copy(a, src, g, q).start()
        if last is not None:
            finish(*last)
            if i == 2 * len(others):
                activate()
                submit(f, 0, True)
                submit(f, 1, True)
        if a == 2:
            submit(src, g, False)
        last = (a, src)
    finish(*last)
    for entry in pending:
        mix(*entry)
    total = mown[...]
    for p in others:
        for half in range(2):
            m_copy(p, half, p).wait_recv()
        total = total + mrecv[p].astype(jnp.float32)
    mo[...] = total.astype(jnp.bfloat16)

    for p in peers:
        t_copy(p, t).wait_send()
        for c in range(F):
            for half in range(2):
                p_copy(c, half, p, t).wait_send()
    for k, p in enumerate(others):
        for a in range(3):
            for q in range(pieces_of[a]):
                z_copy(a, k, p, f, q).wait_send()
                y_copy(a, p, g, q).wait_send()
        for half in range(2):
            m_copy(p, half, f).wait_send()


def exchange(F, T, gate, up, down, gain, tokens, routes, weight):
    R, FF = gate.shape
    C, D, H = FF // F, F * R, R // 2
    Q = 4
    tok, S = tokens.shape[0], EXPERTS * CAP
    bf, f32 = jnp.bfloat16, jnp.float32
    any_spec, vm = pl.BlockSpec(memory_space=pl.ANY), pl.BlockSpec(memory_space=pltpu.VMEM)
    dma = pltpu.SemaphoreType.DMA
    return pl.pallas_call(
        functools.partial(exchange_kernel, F, T, R, C, Q),
        name="exchange",
        out_shape=(pltpu.VMEM((D, C), bf), pltpu.VMEM((D, C), bf),
                   pltpu.VMEM((C, D), bf), jax.ShapeDtypeStruct((tok, R), bf)),
        in_specs=[any_spec] * 3 + [vm] * 5,
        out_specs=(vm, vm, vm, vm),
        scratch_shapes=[
            pltpu.VMEM((3, H, C), f32), pltpu.VMEM((3, C, H), f32),
            pltpu.VMEM((2, F - 1, H, C), bf), pltpu.VMEM((F - 1, C, H), bf),
            pltpu.VMEM((tok, D), bf), pltpu.VMEM((S, D), bf), pltpu.VMEM((tok, S), bf), pltpu.VMEM((tok, S), bf),
            pltpu.VMEM((S, D), bf),
            pltpu.VMEM((S, C), f32), pltpu.VMEM((S, C), f32), pltpu.VMEM((S, C), bf),
            pltpu.VMEM((S, D), bf), pltpu.VMEM((S, D), bf), pltpu.VMEM((tok, D), bf),
            pltpu.VMEM((tok, R), f32), pltpu.VMEM((F, tok, R), bf),
            dma((3, F, Q)), dma((3, F, Q)), dma((3, F, Q)), dma((3, F, Q)), dma((T,)), dma((T,)),
            dma((F, 2, T)), dma((F, 2, T)), dma((F, 2)), dma((F, 2)), dma((6,)),
        ],
        compiler_params=pltpu.CompilerParams(collective_id=0, has_side_effects=True, vmem_limit_bytes=42 * 1024 * 1024),
    )(gate, up, down, gain[:, None], tokens, routes, routes.T, weight)


def fits(grp_count, fs_count, pieces, gate_train):
    rows, wide = gate_train.shape[1:]
    return (grp_count == 2 and fs_count == pieces and fs_count % 2 == 0
            and wide % (fs_count * 128) == 0 and rows % 256 == 0 and 4 <= 2 * fs_count <= 8)


def shards(tokens, routes, route_weight, norm_gain, gate_train, up_train, down_train):
    fs_count = lax.axis_size("fs")
    pieces = min(fs_count, 32)
    copies = fs_count // pieces
    if fits(lax.axis_size("grp"), fs_count, pieces, gate_train):
        gate_new, up_new, down_new, mixed = exchange(
            fs_count, lax.axis_size("tp"), gate_train[0], up_train[0], down_train[0],
            norm_gain, tokens, routes, route_weight,
        )
        return (gate_new[None], up_new[None], down_new[None], mixed)
    gain_column = norm_gain[:, None]
    gate_low = (gate_train[0] * gain_column).astype(jnp.bfloat16)
    up_low = (up_train[0] * gain_column).astype(jnp.bfloat16)
    down_low = down_train[0].astype(jnp.bfloat16)
    gate_wide = jnp.tile(gate_low, (1, copies))
    up_wide = jnp.tile(up_low, (1, copies))
    down_wide = jnp.tile(down_low, (copies, 1))
    gate_new, up_new = (
        lax.all_to_all(gate_wide, "fs", split_axis=1, concat_axis=0, tiled=True),
        lax.all_to_all(up_wide, "fs", split_axis=1, concat_axis=0, tiled=True),
    )
    down_new = lax.all_to_all(down_wide, "fs", split_axis=0, concat_axis=1, tiled=True)
    tok_float = tokens.astype(jnp.float32)
    normed = (
        tok_float * lax.rsqrt(jnp.mean(tok_float * tok_float, axis=-1, keepdims=True) + 1e-06)
    ).astype(jnp.bfloat16)
    chosen = routes.reshape(-1)
    chosen_hot = (chosen[:, None] == jnp.arange(EXPERTS, dtype=jnp.int32)[None, :]).astype(
        jnp.int32
    )
    before = jnp.cumsum(chosen_hot, axis=0) - chosen_hot
    slot_rank = jnp.sum(before * chosen_hot, axis=1)
    slot_index = (chosen * CAP + slot_rank).reshape(routes.shape)
    slot_range = jnp.arange(EXPERTS * CAP, dtype=jnp.int32)
    select_rows = jnp.any(slot_range[:, None, None] == slot_index[None, :, :], axis=-1).astype(
        jnp.bfloat16
    )
    outgoing = jnp.dot(select_rows, normed, preferred_element_type=jnp.float32).astype(jnp.bfloat16)
    outgoing = outgoing.reshape(EXPERTS, CAP, normed.shape[1])
    arrived = lax.all_to_all(outgoing, "tp", split_axis=0, concat_axis=0, tiled=True).reshape(
        EXPERTS * CAP, normed.shape[1]
    )
    slot_count = EXPERTS * CAP // copies
    copy_index = lax.axis_index("fs") // pieces
    my_rows = lax.dynamic_slice_in_dim(arrived, copy_index * slot_count, slot_count, 0)
    gated = jnp.dot(my_rows, gate_new, preferred_element_type=jnp.float32)
    lifted = jnp.dot(my_rows, up_new, preferred_element_type=jnp.float32)
    hidden = (jax.nn.silu(gated) * lifted).astype(jnp.bfloat16)
    partial_out = jnp.dot(hidden, down_new, preferred_element_type=jnp.float32)
    placed = jnp.zeros((EXPERTS * CAP, partial_out.shape[1]), jnp.float32)
    placed = lax.dynamic_update_slice_in_dim(placed, partial_out, copy_index * slot_count, 0)
    expert_out = lax.psum_scatter(placed, "fs", scatter_dimension=1, tiled=True).astype(
        jnp.bfloat16
    )
    returned = lax.all_to_all(
        expert_out.reshape(EXPERTS, CAP, expert_out.shape[1]),
        "tp",
        split_axis=0,
        concat_axis=0,
        tiled=True,
    )
    returned = returned.reshape(EXPERTS * CAP, expert_out.shape[1]).astype(jnp.float32)
    blend_weight = jnp.sum(
        jnp.where(
            slot_range[None, None, :] == slot_index[:, :, None], route_weight[:, :, None], 0.0
        ),
        axis=1,
    )
    mixed = jnp.dot(
        blend_weight, returned, precision=lax.Precision.HIGHEST, preferred_element_type=jnp.float32
    )
    return (gate_new[None], up_new[None], down_new[None], mixed.astype(jnp.bfloat16))


def solution(mesh):
    in_specs = (
        P(("grp", "tp"), None),
        P(("grp", "tp"), None),
        P(("grp", "tp"), None),
        P("fs"),
        P("tp", "fs", None),
        P("tp", "fs", None),
        P("tp", None, "fs"),
    )
    out_specs = (
        P(("grp", "tp"), None, "fs"),
        P(("grp", "tp"), None, "fs"),
        P(("grp", "tp"), "fs", None),
        P(("grp", "tp"), "fs"),
    )
    return jax.shard_map(shards, mesh=mesh, in_specs=in_specs, out_specs=out_specs, check_vma=False)
```

time: 297 us -> 270 us (0.909)
  other arithmetic: 26.1 us -> 0 us
  Pallas kernels: 247 us -> 251 us
  matrix products: 3.3 us -> 0 us
    convert_element_type x4 -> x0, other arithmetic: 21.5 us -> none  [the longest x1 13.2 us: shards(): up_low = (up_train[0] * gain_column).astype(jnp.bfloat16)]
    pallas_call x1, Pallas kernels: 247 us -> 251 us  [exchange(): pl.pallas_call(functools.partial(exchange_kernel, F, T, R, C, Q), name='e...]
    dot_general x1 -> x0, matrix products: 3.3 us -> none  [shards(): jnp.dot(select_rows, normed, preferred_element_type=jnp.float32)]
    unnamed x15 -> x8, local copies, waits for them, and re-layouts: 14.3 us -> 11.2 us
where the time goes in v2:
time: 270 us; the launch traced here: 264 us
  Pallas kernels  251 us (93%)
  local copies, waits for them, and re-layouts  12.7 us (5%)
    pallas_call x1, Pallas kernels, exchange(): pl.pallas_call(functools.partial(exchange_kernel, F, T, R, C, Q), name='e...  251 us
    unnamed x8, local copies, waits for them, and re-layouts  11.2 us

profile of v2, /device:TPU:13, one launch (start us, length us, event | category | flops | bytes accessed | tf_op | source)
XLA Modules:
  0.0 264.3 jit_solution(6747957347894279135)
XLA Ops:
  0.6 1.4 copy.15.weight
  2.1 1.4 copy.14.routes
  3.5 1.5 copy.13.gain
  5.1 250.9 %exchange.1 = (bf16[2048,1408]{1,0:T(8,128)(2,1)S(1)}, bf16[2048,1408]{1,0:T(8,128)(2,1)S(1)}, bf16[1408,2048]{1,0:T(8,128)(2,1)S(1)}, bf16[192,512]{1,0:T(8,128)(2,1)}) custom-call(f32[512,5632]{1,0:T(8,128)} %bitcast.11, f32[512,5632]{1,0:T(8,128)} %bitcast.12, f32[5632,512]{1,0:T(8,128)} %bitcast.13, f32[512,1]{1,0:T(8,128)} %copy.13.gain, ...), custom_call_target="tpu_custom_call" | custom-call | tf_op jit(solution)/shard_map/exchange/pallas_call | solution.py:291
  256.0 2.5 copy.20
  258.5 2.5 copy.21
  261.0 0.0 copy-start
  261.0 2.5 copy.22
  263.6 0.0 copy-done
  263.6 0.7 copy.23
Async XLA Ops:
  261.0 2.5 copy-start

commit v3 on v2

--- a/solution.py
+++ b/solution.py
@@ -11,8 +11,8 @@
 MESH = pl.DeviceIdType.MESH
 
 
-def exchange_kernel(F, T, R, C, Q, gt, ut, dt, gain, tokens, routes, routes_t, weight, gw, uw, dw, mo,
-                    wide, tall, sendw, sendt, normed, xs, bh, bl,
+def exchange_kernel(F, T, R, C, Q, gt, ut, dt, gain, tokens, routes_t, weight_t, gw, uw, dw, mo,
+                    flat, turned, scale_at, wide, tall, sendw, sendt, normed, xs, bh, bl,
                     arr, gacc, uacc, hid, pbf, ret, msend, mown, mrecv,
                     zs, zr, ys, yr, ts, tr, ps, pr, ms, mr, loc):
     g, f, t = lax.axis_index("grp"), lax.axis_index("fs"), lax.axis_index("tp")
@@ -82,7 +82,11 @@
             send_sem=ms.at[tgt, half], recv_sem=mr.at[src, half],
             device_id={"fs": tgt}, device_id_type=MESH)
 
-    tasks = [(a, k, g) for a in range(3) for k in range(len(others))]
+    if len(others) == 3:
+        order = [(0, 0), (0, 1), (0, 2), (1, 0), (1, 2), (2, 2), (1, 1), (2, 0), (2, 1)]
+    else:
+        order = [(a, k) for a in range(3) for k in range(len(others))]
+    tasks = [(a, k, g) for a, k in order]
     tasks += [(a, None, half) for a in range(3) for half in range(2)]
 
     def stage_copy(n):
@@ -100,7 +104,7 @@
             @pl.loop(0, H // 32)
             def _(m):
                 rows = pl.ds(pl.multiple_of(m * 32, 32), 32)
-                scale = gain[pl.ds(pl.multiple_of(half * H + m * 32, 32), 32), :]
+                scale = scale_at[pl.ds(pl.multiple_of(half * H + m * 32, 32), 32), 0:1]
                 value = (wide[n % 3, rows, :] * scale).astype(jnp.bfloat16)
                 if k is None:
                     wins[a][pl.ds(pl.multiple_of(f * R + half * H + m * 32, 32), 32), :] = value
@@ -129,36 +133,38 @@
                 value * lax.rsqrt(jnp.mean(value * value, axis=-1, keepdims=True) + 1e-06)
             ).astype(jnp.bfloat16)
 
-        def ranks(shape, axis, one, two, hot_first, earlier):
-            expert = lax.broadcasted_iota(jnp.int32, shape, axis)
-            hot = jnp.where((expert == one) | (expert == two), 1.0, 0.0).astype(jnp.bfloat16)
-            order = (hot, earlier) if hot_first else (earlier, hot)
-            before = jnp.dot(*order, preferred_element_type=jnp.float32)
-            return [
-                name.astype(jnp.float32) * CAP
-                + jnp.sum(jnp.where(expert == name, before, 0.0), axis=axis, keepdims=True)
-                for name in (one, two)
-            ]
-
+        one, two = routes_t[0:1, :], routes_t[1:2, :]
         row = lax.broadcasted_iota(jnp.int32, (tok, tok), 0)
         col = lax.broadcasted_iota(jnp.int32, (tok, tok), 1)
-        first, second = ranks((16, tok), 0, routes_t[0:1, :], routes_t[1:2, :], True,
-                              jnp.where(row < col, 1.0, 0.0).astype(jnp.bfloat16))
+        expert = lax.broadcasted_iota(jnp.int32, (16, tok), 0)
+        hot = jnp.where((expert == one) | (expert == two), 1.0, 0.0).astype(jnp.bfloat16)
+        before = jnp.dot(hot, jnp.where(row < col, 1.0, 0.0).astype(jnp.bfloat16), preferred_element_type=jnp.float32)
+        first, second = [
+            name.astype(jnp.float32) * CAP
+            + jnp.sum(jnp.where(expert == name, before, 0.0), axis=0, keepdims=True)
+            for name in (one, two)
+        ]
         slot = lax.broadcasted_iota(jnp.int32, (slot_all, tok), 0).astype(jnp.float32)
         select = jnp.where((slot == first) | (slot == second), 1.0, 0.0).astype(jnp.bfloat16)
         for n in range(4):
             cols = pl.ds(n * (F * R // 4), F * R // 4)
             xs[:, cols] = jnp.dot(select, normed[:, cols], preferred_element_type=jnp.float32).astype(jnp.bfloat16)
-        first, second = ranks((tok, 128), 1, routes[:, 0:1], routes[:, 1:2], False,
-                              jnp.where(row > col, 1.0, 0.0).astype(jnp.bfloat16))
+        flat[...] = jnp.zeros_like(flat)
+        for n, line in enumerate((first, second, weight_t[0:1, :], weight_t[1:2, :])):
+            flat[n:n + 1, 0:tok] = line
+        turned[...] = flat[...].T
         slot = lax.broadcasted_iota(jnp.int32, (tok, slot_all), 1).astype(jnp.float32)
-        blend = jnp.where(slot == first, weight[:, 0:1], 0.0) + jnp.where(slot == second, weight[:, 1:2], 0.0)
+        blend = jnp.where(slot == turned[0:tok, 0:1], turned[0:tok, 2:3], 0.0) + jnp.where(
+            slot == turned[0:tok, 1:2], turned[0:tok, 3:4], 0.0)
         high = blend.astype(jnp.bfloat16)
         bh[...] = high
         bl[...] = (blend - high.astype(jnp.float32)).astype(jnp.bfloat16)
 
     for n in range(3):
         stage_copy(n).start()
+    for n in range(R // 128):
+        piece = pl.ds(n * 128, 128)
+        scale_at[piece, :] = jnp.broadcast_to(gain[0:1, piece], (128, 128)).T
     remote = 3 * len(others)
     for n in range(remote):
         cast(n)
@@ -239,24 +245,37 @@
         if a < 2:
             multiply(a, src, False)
         else:
-            submit(src, 1 - g, False)
-
-    items = [(a, src) for a in (0, 1) for src in others] + [(2, src) for src in others]
+            offer(src, 1 - g)
+
+    waiting, done = [], []
+
+    def offer(src, half):
+        waiting.append((src, half, False))
+        if len(done) == 2 * len(others):
+            while waiting:
+                submit(*waiting.pop(0))
+
+    def settle(a, src):
+        finish(a, src)
+        if a < 2:
+            done.append(src)
+            if len(done) == 2 * len(others):
+                activate()
+                submit(f, 0, True)
+                submit(f, 1, True)
+
+    items = [(a, others[k]) for a, k in order]
     last = None
-    for i, (a, src) in enumerate(items):
+    for a, src in items:
         for q in range(pieces_of[a]):
             z_recv(a, src, q).wait_recv()
             y_copy(a, src, g, q).start()
         if last is not None:
-            finish(*last)
-            if i == 2 * len(others):
-                activate()
-                submit(f, 0, True)
-                submit(f, 1, True)
+            settle(*last)
         if a == 2:
-            submit(src, g, False)
+            offer(src, g)
         last = (a, src)
-    finish(*last)
+    settle(*last)
     for entry in pending:
         mix(*entry)
     total = mown[...]
@@ -281,6 +300,7 @@
 
 
 def exchange(F, T, gate, up, down, gain, tokens, routes, weight):
+    span = -(-tokens.shape[0] // 128) * 128
     R, FF = gate.shape
     C, D, H = FF // F, F * R, R // 2
     Q = 4
@@ -293,9 +313,10 @@
         name="exchange",
         out_shape=(pltpu.VMEM((D, C), bf), pltpu.VMEM((D, C), bf),
                    pltpu.VMEM((C, D), bf), jax.ShapeDtypeStruct((tok, R), bf)),
-        in_specs=[any_spec] * 3 + [vm] * 5,
+        in_specs=[any_spec] * 3 + [vm] * 4,
         out_specs=(vm, vm, vm, vm),
         scratch_shapes=[
+            pltpu.VMEM((128, span), f32), pltpu.VMEM((span, 128), f32), pltpu.VMEM((R, 128), f32),
             pltpu.VMEM((3, H, C), f32), pltpu.VMEM((3, C, H), f32),
             pltpu.VMEM((2, F - 1, H, C), bf), pltpu.VMEM((F - 1, C, H), bf),
             pltpu.VMEM((tok, D), bf), pltpu.VMEM((S, D), bf), pltpu.VMEM((tok, S), bf), pltpu.VMEM((tok, S), bf),
@@ -307,7 +328,7 @@
             dma((F, 2, T)), dma((F, 2, T)), dma((F, 2)), dma((F, 2)), dma((6,)),
         ],
         compiler_params=pltpu.CompilerParams(collective_id=0, has_side_effects=True, vmem_limit_bytes=42 * 1024 * 1024),
-    )(gate, up, down, gain[:, None], tokens, routes, routes.T, weight)
+    )(gate, up, down, gain[None, :], tokens, routes.T, weight.T)
 
 
 def fits(grp_count, fs_count, pieces, gate_train):

time: 270 us -> 236 us (0.87); the launches traced: 264 us -> 236 us
  Pallas kernels: 251 us -> 227 us
  local copies, waits for them, and re-layouts: 12.7 us -> 8.27 us
    pallas_call x1, Pallas kernels: 251 us -> 227 us  [exchange(): pl.pallas_call(functools.partial(exchange_kernel, F, T, R, C, Q), name='e...]
    unnamed x8 -> x6, local copies, waits for them, and re-layouts: 11.2 us -> 8.27 us
where the time goes in v3:
time: 236 us
  Pallas kernels  227 us (96%)
  local copies, waits for them, and re-layouts  8.27 us (4%)
    pallas_call x1, Pallas kernels, exchange(): pl.pallas_call(functools.partial(exchange_kernel, F, T, R, C, Q), name='e...  227 us
    unnamed x6, local copies, waits for them, and re-layouts  8.27 us

profile of v3, /device:TPU:13, one launch (start us, length us, event | category | flops | bytes accessed | tf_op | source)
XLA Modules:
  0.0 235.5 jit_solution(6881161125158670626)
XLA Ops:
  0.6 226.6 %exchange.1 = (bf16[2048,1408]{1,0:T(8,128)(2,1)S(1)}, bf16[2048,1408]{1,0:T(8,128)(2,1)S(1)}, bf16[1408,2048]{1,0:T(8,128)(2,1)S(1)}, bf16[192,512]{1,0:T(8,128)(2,1)}) custom-call(f32[512,5632]{1,0:T(8,128)} %bitcast.12, f32[512,5632]{1,0:T(8,128)} %bitcast.13, f32[5632,512]{1,0:T(8,128)} %bitcast.14, f32[1,512]{1,0:T(1,128)} %bitcast.15, ...), custom_call_target="tpu_custom_call" | custom-call | tf_op jit(solution)/shard_map/exchange/pallas_call | solution.py:311
  227.2 2.5 %copy.15 = bf16[1,2048,1408]{2,1,0:T(8,128)(2,1)} copy(bf16[1,2048,1408]{2,1,0:T(8,128)(2,1)S(1)} %bitcast.11) | data formatting | bytes 11534336
  229.8 2.5 %copy.16 = bf16[1,2048,1408]{2,1,0:T(8,128)(2,1)} copy(bf16[1,2048,1408]{2,1,0:T(8,128)(2,1)S(1)} %bitcast.10) | data formatting | bytes 11534336
  232.3 0.0 copy-start
  232.3 2.5 %copy.17 = bf16[1,1408,2048]{2,1,0:T(8,128)(2,1)} copy(bf16[1,1408,2048]{2,1,0:T(8,128)(2,1)S(1)} %bitcast.9) | data formatting | bytes 11534336
  234.8 0.0 copy-done
  234.8 0.7 copy.18
Async XLA Ops:
  232.3 2.5 %copy-start = (bf16[192,512]{1,0:T(8,128)(2,1)S(1)}, bf16[192,512]{1,0:T(8,128)(2,1)}, u32[]{:S(2)}) copy-start(bf16[192,512]{1,0:T(8,128)(2,1)} %get-tuple-element.23) | copy-start | bytes 589828
